TPU v7x, 32 devices: a whole 2x2x4 slice. The times are simulated.
32 devices in a mesh: grp: 2 (over y), fs: 4 (over z), tp: 4 (over x, core).
Axes of the slice: x: 2, y: 2, z: 4, core: 2. Of those that a mesh axis runs over, the one named last changes fastest.
Arguments:
- tokens: bfloat16 [2048, 2048], P(('grp', 'fs')), parts along dimension 0, may hold values from -6 to 6
- ffn_pre_gain: bfloat16 [2048], replicated, may hold values from 0.099609375 to 1.8984375
- gate_weight: bfloat16 [2048, 5632], P('fs', 'tp'), may hold values from -0.125 to 0.125
- up_weight: bfloat16 [2048, 5632], P('fs', 'tp'), may hold values from -0.125 to 0.125
- down_weight: bfloat16 [5632, 2048], P('tp', 'fs'), may hold values from -0.078125 to 0.078125
- ffn_post_gain: bfloat16 [2048], replicated, may hold values from 0.099609375 to 1.8984375
- mix_pre_gain: bfloat16 [2048], replicated, may hold values from 0.099609375 to 1.8984375
- mix_u_weight: bfloat16 [2048, 2048], P('fs', 'tp'), may hold values from -0.125 to 0.125
- mix_v_weight: bfloat16 [2048, 2048], P('fs', 'tp'), may hold values from -0.125 to 0.125
- spatial_gain: bfloat16 [2048], P('tp'), may hold values from 0.099609375 to 1.8984375
- spatial_weight: bfloat16 [16, 128, 128], P('tp'), may hold values from -0.5 to 0.5
- spatial_bias: bfloat16 [16, 128], P('tp'), may hold values from 0.099609375 to 1.8984375
- mix_out_weight: bfloat16 [2048, 2048], P('tp', 'fs'), may hold values from -0.125 to 0.125
- mix_post_gain: bfloat16 [2048], replicated, may hold values from 0.099609375 to 1.8984375
- late_pre_gain: bfloat16 [2048], replicated, may hold values from 0.099609375 to 1.8984375
- late_post_gain: bfloat16 [2048], replicated, may hold values from 0.099609375 to 1.8984375
Outputs:
- result: bfloat16 [2048, 2048], P(('grp', 'fs')), parts along dimension 0
There are 2 independent parts, one for each index of `grp`. A program takes and returns all parts, laid end to end along the dimension named above; an argument that names none is the same for every part. Nothing has to cross between parts.
All inputs are finite; a program needn't handle non-finite values.
Results may differ from a plain program's by a relative error of at most 0.019.
Values may be sent and summed in bfloat16 or wider, within the bound.
No kernel may reach another device: no remote copies, remote signals or barrier semaphores. Data moves between devices by JAX's collectives and lax.ppermute only.
A program may use at most 128 MiB of HBM per device.

v0:
```python
import jax
import jax.numpy as jnp
from jax import lax
from jax.sharding import PartitionSpec as P

GROUP_WIDTH = 128
BLOCK = 128


def row_norm(values, gain):
    scale = lax.rsqrt(jnp.mean(values * values, axis=-1, keepdims=True) + 1e-06)
    return values * scale * gain.astype(jnp.float32)


def reduce_partial(terms):
    return lax.psum(terms.astype(jnp.bfloat16), "tp").astype(jnp.float32)


def add_branch(stream, terms, gain, factor):
    total = reduce_partial(terms)
    return (stream.astype(jnp.float32) + factor * row_norm(total, gain)).astype(jnp.bfloat16)


def gated_hidden(normed, gate_full, up_full):
    gate = jnp.dot(normed, gate_full, preferred_element_type=jnp.float32)
    upper = jnp.dot(normed, up_full, preferred_element_type=jnp.float32)
    return (jax.nn.silu(gate) * upper).astype(jnp.bfloat16)


def spatial_mix(u_linear, v_linear, spatial_gain, spatial_weight, spatial_bias):
    count = u_linear.shape[0]
    gated_u = jax.nn.gelu(u_linear, approximate=False)
    gating_v = jax.nn.gelu(v_linear, approximate=False)
    groups = gating_v.shape[1] // GROUP_WIDTH
    grouped = gating_v.reshape(count, groups, GROUP_WIDTH)
    centred = grouped - jnp.mean(grouped, axis=-1, keepdims=True)
    vnorm = centred * lax.rsqrt(jnp.mean(centred * centred, axis=-1, keepdims=True) + 1e-05)
    vnorm = (vnorm * spatial_gain.astype(jnp.float32).reshape(groups, GROUP_WIDTH)).astype(
        jnp.bfloat16
    )
    blocks = vnorm.reshape(count // BLOCK, BLOCK, groups, GROUP_WIDTH)
    lower = jnp.tril(jnp.ones((BLOCK, BLOCK), dtype=bool))
    masked = jnp.where(lower[None], spatial_weight, jnp.zeros_like(spatial_weight))
    spatial = jnp.einsum("gts,nsgc->ntgc", masked, blocks, preferred_element_type=jnp.float32)
    spatial = spatial + spatial_bias.astype(jnp.float32).T[None, :, :, None]
    return (gated_u * spatial.reshape(count, groups * GROUP_WIDTH)).astype(jnp.bfloat16)


def shards(
    tokens,
    ffn_pre_gain,
    gate_weight,
    up_weight,
    down_weight,
    ffn_post_gain,
    mix_pre_gain,
    mix_u_weight,
    mix_v_weight,
    spatial_gain,
    spatial_weight,
    spatial_bias,
    mix_out_weight,
    mix_post_gain,
    late_pre_gain,
    late_post_gain,
):
    normed = row_norm(tokens.astype(jnp.float32), ffn_pre_gain).astype(jnp.bfloat16)
    gate_full, up_full = (
        lax.all_gather(gate_weight, "fs", axis=0, tiled=True),
        lax.all_gather(up_weight, "fs", axis=0, tiled=True),
    )
    down_full = lax.all_gather(down_weight, "fs", axis=1, tiled=True)
    hidden = gated_hidden(normed, gate_full, up_full)
    terms = jnp.dot(hidden, down_full, preferred_element_type=jnp.float32)
    first = add_branch(tokens, terms, ffn_post_gain, 0.5)
    normed = row_norm(first.astype(jnp.float32), mix_pre_gain).astype(jnp.bfloat16)
    u_full, v_full = (
        lax.all_gather(mix_u_weight, "fs", axis=0, tiled=True),
        lax.all_gather(mix_v_weight, "fs", axis=0, tiled=True),
    )
    u_linear = jnp.dot(normed, u_full, preferred_element_type=jnp.float32)
    v_linear = jnp.dot(normed, v_full, preferred_element_type=jnp.float32)
    mixed = spatial_mix(u_linear, v_linear, spatial_gain, spatial_weight, spatial_bias)
    out_full = lax.all_gather(mix_out_weight, "fs", axis=1, tiled=True)
    terms = jnp.dot(mixed, out_full, preferred_element_type=jnp.float32)
    second = add_branch(first, terms, mix_post_gain, 1.0)
    normed = row_norm(second.astype(jnp.float32), late_pre_gain).astype(jnp.bfloat16)
    hidden = gated_hidden(normed, gate_full, up_full)
    terms = jnp.dot(hidden, down_full, preferred_element_type=jnp.float32)
    return add_branch(second, terms, late_post_gain, 0.5)


def solution(mesh):
    in_specs = (
        P(("grp", "fs"), None),
        P(),
        P("fs", "tp"),
        P("fs", "tp"),
        P("tp", "fs"),
        P(),
        P(),
        P("fs", "tp"),
        P("fs", "tp"),
        P("tp"),
        P("tp", None, None),
        P("tp", None),
        P("tp", "fs"),
        P(),
        P(),
        P(),
    )
    out_specs = P(("grp", "fs"), None)
    return jax.shard_map(shards, mesh=mesh, in_specs=in_specs, out_specs=out_specs, check_vma=False)
```

profile of v0, /device:TPU:0, one launch (start us, length us, event | category | flops | bytes accessed | tf_op | source)
XLA Modules:
  0.0 620.2 jit_solution(5151979985591970159)
XLA Ops:
  6.5 0.0 copy-start.2
  6.5 0.0 copy-start
  6.5 0.0 all-gather.7.cloned.1.call-start
  6.5 0.7 all-gather.7.cloned.1.call-update
  7.3 0.0 all-gather.11.cloned.1.call-start
  7.3 0.7 all-gather.11.cloned.1.call-update
  8.0 0.0 all-gather.9.cloned.1.call-start
  8.1 0.7 all-gather.9.cloned.1.call-update
  8.7 0.0 all-reduce.4.cloned.1.call-start
  8.8 0.0 copy-done.2
  8.8 0.0 copy-done
  8.8 0.3 fusion.10
  9.1 109.2 %all-gather.7.cloned.1.call-done = bf16[2048,1408]{1,0:T(8,128)(2,1)} async-done(((bf16[512,1408]{1,0:T(8,128)(2,1)}), bf16[2048,1408]{1,0:T(8,128)(2,1)}) %all-gather.7.cloned.1.call-update) | async-done | bytes 5767184 | tf_op jit(solution)/shard_map/all_gather | solution.py:69
  118.3 4.5 fusion.59
  122.8 102.0 %all-gather.11.cloned.1.call-done = bf16[1408,2048]{1,0:T(8,128)(2,1)} async-done(((bf16[1408,512]{1,0:T(8,128)(2,1)}), bf16[1408,2048]{1,0:T(8,128)(2,1)}) %all-gather.11.cloned.1.call-update) | async-done | bytes 5767184 | tf_op jit(solution)/shard_map/all_gather | solution.py:72
  224.9 106.6 %all-gather.9.cloned.1.call-done = bf16[2048,1408]{1,0:T(8,128)(2,1)} async-done(((bf16[512,1408]{1,0:T(8,128)(2,1)}), bf16[2048,1408]{1,0:T(8,128)(2,1)}) %all-gather.9.cloned.1.call-update) | async-done | bytes 5767184 | tf_op jit(solution)/shard_map/all_gather | solution.py:70
  331.4 8.9 %convolution_convert_fusion.2 = bf16[256,2048]{1,0:T(8,128)(2,1)} fusion(bf16[1408,2048]{1,0:T(8,128)(2,1)} %all-gather.11.cloned.1.call-done, bf16[2048,1408]{1,0:T(8,128)(2,1)} %all-gather.9.cloned.1.call-done, f32[256,1408]{1,0:T(8,128)S(1)} %fusion.59, bf16[256,2048]{1,0:T(8,128)(2,1)S(1)} %copy-done, f32[2048]{0:T(1024)S(1)} %convert_element_type.82, ...), kind=kOutput, calls=%fused_computation.21 | convolution fusion | flops 2957574144 | bytes 15082496 | tf_op jit(solution)/shard_map/dot_general | solution.py:74
  340.4 0.0 copy-start.3
  340.4 0.0 all-reduce.4.cloned.1.call-update
  340.4 0.0 all-gather.15.cloned.1.call-start
  340.5 0.5 all-gather.15.cloned.1.call-update
  341.0 0.0 all-gather.13.cloned.1.call-start
  341.0 0.5 all-gather.13.cloned.1.call-update
  341.6 0.0 all-gather.17.cloned.1.call-start
  341.6 0.7 all-gather.17.cloned.1.call-update
  342.3 0.2 all-reduce.6.cloned.1.call-start
  342.6 0.0 copy-done.3
  342.6 0.0 copy-done.4
  342.6 0.0 copy-done.8
  342.6 0.0 copy-done.9
  342.7 32.4 %all-reduce.4.cloned.1.call-done = bf16[256,2048]{1,0:T(8,128)(2,1)} async-done(((bf16[256,2048]{1,0:T(8,128)(2,1)}), bf16[256,2048]{1,0:T(8,128)(2,1)}) %all-reduce.4.cloned.1.call-update) | async-done | bytes 1048592 | tf_op jit(solution)/shard_map/psum | solution.py:16
  375.1 1.5 fusion.2
  376.6 2.0 fusion.14
  378.6 44.1 %all-gather.15.cloned.1.call-done = bf16[2048,512]{1,0:T(8,128)(2,1)} async-done(((bf16[512,512]{1,0:T(8,128)(2,1)}), bf16[2048,512]{1,0:T(8,128)(2,1)}) %all-gather.15.cloned.1.call-update) | async-done | bytes 2097168 | tf_op jit(solution)/shard_map/all_gather | solution.py:79
  422.7 3.4 fusion.28
  426.1 0.2 reshape.99
  426.3 0.0 copy-start.1
  426.3 0.2 reshape.98
  426.5 0.3 reduce_sum.75
  426.8 0.6 multiply_reduce_fusion
  427.5 0.1 copy.36
  427.6 0.1 copy.37
  427.7 0.2 copy.25
  427.9 0.0 copy-done.1
  427.9 0.3 fusion.22
  428.2 0.2 copy.28
  428.5 40.1 %all-gather.13.cloned.1.call-done = bf16[2048,512]{1,0:T(8,128)(2,1)} async-done(((bf16[512,512]{1,0:T(8,128)(2,1)}), bf16[2048,512]{1,0:T(8,128)(2,1)}) %all-gather.13.cloned.1.call-update) | async-done | bytes 2097168 | tf_op jit(solution)/shard_map/all_gather | solution.py:78
  468.6 46.1 %all-gather.17.cloned.1.call-done = bf16[512,2048]{1,0:T(8,128)(2,1)} async-done(((bf16[512,512]{1,0:T(8,128)(2,1)}), bf16[512,2048]{1,0:T(8,128)(2,1)}) %all-gather.17.cloned.1.call-update) | async-done | bytes 2097168 | tf_op jit(solution)/shard_map/all_gather | solution.py:84
  514.7 5.7 convolution_convert_fusion
  520.4 0.0 all-reduce.6.cloned.1.call-update
  520.4 0.3 all-reduce.8.cloned.1.call-start
  520.7 0.0 copy-done.5
  520.7 0.0 copy-done.6
  520.7 34.9 %all-reduce.6.cloned.1.call-done = bf16[256,2048]{1,0:T(8,128)(2,1)} async-done(((bf16[256,2048]{1,0:T(8,128)(2,1)}), bf16[256,2048]{1,0:T(8,128)(2,1)}) %all-reduce.6.cloned.1.call-update) | async-done | bytes 1048592 | tf_op jit(solution)/shard_map/psum | solution.py:16
  555.7 1.5 fusion.5
  557.2 1.9 fusion.18
  559.1 4.5 fusion.45
  563.6 0.0 copy-start.7
  563.6 8.9 %convolution_convert_fusion.1 = bf16[256,2048]{1,0:T(8,128)(2,1)} fusion(bf16[1408,2048]{1,0:T(8,128)(2,1)} %all-gather.11.cloned.1.call-done, bf16[2048,1408]{1,0:T(8,128)(2,1)} %all-gather.9.cloned.1.call-done, f32[256,1408]{1,0:T(8,128)S(1)} %fusion.45, bf16[256,2048]{1,0:T(8,128)(2,1)S(1)} %get-tuple-element.6, f32[2048]{0:T(1024)S(1)} %convert_element_type.99, ...), kind=kOutput, calls=%fused_computation.20 | convolution fusion | flops 2957574144 | bytes 15082496 | tf_op jit(solution)/shard_map/dot_general | solution.py:89
  572.5 0.0 all-reduce.8.cloned.1.call-update
  572.5 0.0 copy-done.7
  572.5 36.9 %all-reduce.8.cloned.1.call-done = bf16[256,2048]{1,0:T(8,128)(2,1)} async-done(((bf16[256,2048]{1,0:T(8,128)(2,1)}), bf16[256,2048]{1,0:T(8,128)(2,1)}) %all-reduce.8.cloned.1.call-update) | async-done | bytes 1048592 | tf_op jit(solution)/shard_map/psum | solution.py:16
  609.4 1.5 fusion.7
  610.9 2.8 fusion.21
  (22 shorter events, 0.1 us)
Async XLA Ops:
  6.5 2.3 copy-start.2
  6.5 2.3 copy-start
  6.5 111.8 %all-gather.7.cloned.1.call-start = ((), (), s32[]{:S(2)}) async-start(), calls=%async_computation | async-start | bytes 7208960 | tf_op jit(solution)/shard_map/all_gather | solution.py:69
  7.3 217.6 %all-gather.11.cloned.1.call-start = ((), (), s32[]{:S(2)}) async-start(), calls=%async_computation.2 | async-start | bytes 7208960 | tf_op jit(solution)/shard_map/all_gather | solution.py:72
  8.0 323.4 %all-gather.9.cloned.1.call-start = ((), (), s32[]{:S(2)}) async-start(), calls=%async_computation.1 | async-start | bytes 7208960 | tf_op jit(solution)/shard_map/all_gather | solution.py:70
  8.7 366.4 %all-reduce.4.cloned.1.call-start = ((), (), s32[]{:S(2)}) async-start(), calls=%async_computation.3 | async-start | bytes 2097152 | tf_op jit(solution)/shard_map/psum | solution.py:16
  340.4 2.2 copy-start.3
  340.4 2.2 copy-start.4
  340.4 2.2 copy-start.8
  340.4 2.3 copy-start.9
  340.4 82.3 %all-gather.15.cloned.1.call-start = ((), (), s32[]{:S(2)}) async-start(), calls=%async_computation.5 | async-start | bytes 2621440 | tf_op jit(solution)/shard_map/all_gather | solution.py:79
  341.0 127.6 %all-gather.13.cloned.1.call-start = ((), (), s32[]{:S(2)}) async-start(), calls=%async_computation.4 | async-start | bytes 2621440 | tf_op jit(solution)/shard_map/all_gather | solution.py:78
  341.6 173.1 %all-gather.17.cloned.1.call-start = ((), (), s32[]{:S(2)}) async-start(), calls=%async_computation.6 | async-start | bytes 2621440 | tf_op jit(solution)/shard_map/all_gather | solution.py:84
  342.3 213.3 %all-reduce.6.cloned.1.call-start = ((), (), s32[]{:S(2)}) async-start(), calls=%async_computation.7 | async-start | bytes 2097152 | tf_op jit(solution)/shard_map/psum | solution.py:16
  426.3 1.7 copy-start.1
  514.7 6.0 copy-start.5
  514.7 6.0 copy-start.6
  520.4 89.0 %all-reduce.8.cloned.1.call-start = ((), (), s32[]{:S(2)}) async-start(), calls=%async_computation.8 | async-start | bytes 2097152 | tf_op jit(solution)/shard_map/psum | solution.py:16
  563.6 9.0 %copy-start.7 = (bf16[2048]{0:T(1024)(128)(2,1)S(1)}, bf16[2048]{0:T(1024)(128)(2,1)}, u32[]{:S(2)}) copy-start(bf16[2048]{0:T(1024)(128)(2,1)} %param.31) | copy-start | bytes 12292
Sparse Core Ops, SparseCore 0:
  8.9 109.3 all-gather.6
  119.9 104.9 all-gather.10
  226.5 104.9 all-gather.8
  340.5 34.5 all-reduce.3
  376.5 46.1 all-gather.14
  424.1 44.4 all-gather.12
  470.2 44.4 all-gather.16
  520.5 35.0 all-reduce.5
  572.6 36.7 all-reduce.7
where the time goes:
time: 621 us; the launch traced here: 620 us
  waiting for transfers between devices  556 us (90%)
  matrix products  36.2 us (6%)
  between operations  13.5 us (2%)
  other arithmetic  12.6 us (2%)
    all_gather x1, waiting for transfers between devices, shards(): lax.all_gather(gate_weight, 'fs', axis=0, tiled=True)  109 us
    all_gather x1, waiting for transfers between devices, shards(): lax.all_gather(up_weight, 'fs', axis=0, tiled=True)  107 us
    psum x3, waiting for transfers between devices, reduce_partial(): return lax.psum(terms.astype(jnp.bfloat16), 'tp').astype(jnp.float32)  104 us
    all_gather x1, waiting for transfers between devices, shards(): down_full = lax.all_gather(down_weight, 'fs', axis=1, tiled=True)  102 us
    all_gather x1, waiting for transfers between devices, shards(): out_full = lax.all_gather(mix_out_weight, 'fs', axis=1, tiled=True)  46.1 us
    all_gather x1, waiting for transfers between devices, shards(): lax.all_gather(mix_v_weight, 'fs', axis=0, tiled=True)  44.1 us
    all_gather x1, waiting for transfers between devices, shards(): lax.all_gather(mix_u_weight, 'fs', axis=0, tiled=True)  40.1 us
    dot_general x2, matrix products, shards(): terms = jnp.dot(hidden, down_full, preferred_element_type=jnp.float32)  17.8 us
  transfers between devices with their start and end apart: 9, of which 9 were waited for; matrix products, arithmetic and copies ran while one was open for 2% of the time, Pallas kernels for 0%

commit v1 on v0

--- a/solution.py
+++ b/solution.py
@@ -1,3 +1,4 @@
+import functools
 import jax
 import jax.numpy as jnp
 from jax import lax
@@ -5,6 +6,16 @@
 
 GROUP_WIDTH = 128
 BLOCK = 128
+
+
+def get_the_levels_all(body, join_dim):
+    aux = jax.lax.axis_size("fs")
+    v1 = jnp.stack([body] * aux)
+    view_out = jax.lax.all_to_all(v1, "fs", 0, 0)
+    return jnp.concatenate(view_out, axis=join_dim)
+
+
+open_slices = functools.partial(get_the_levels_all, join_dim=0)
 
 
 def row_norm(values, gain):
@@ -76,7 +87,7 @@
     normed = row_norm(first.astype(jnp.float32), mix_pre_gain).astype(jnp.bfloat16)
     u_full, v_full = (
         lax.all_gather(mix_u_weight, "fs", axis=0, tiled=True),
-        lax.all_gather(mix_v_weight, "fs", axis=0, tiled=True),
+        open_slices(mix_v_weight),
     )
     u_linear = jnp.dot(normed, u_full, preferred_element_type=jnp.float32)
     v_linear = jnp.dot(normed, v_full, preferred_element_type=jnp.float32)

time: 621 us -> 582 us (0.937)
  waiting for transfers between devices: 556 us -> 512 us
    all_gather x1 -> x0, waiting for transfers between devices: 44.1 us -> none  [shards(): lax.all_gather(mix_v_weight, 'fs', axis=0, tiled=True)]
    all_to_all x0 -> x1, waiting for transfers between devices: none -> 37.9 us  [get_the_levels_all(): view_out = jax.lax.all_to_all(v1, 'fs', 0, 0)]
    all_gather x1, waiting for transfers between devices: 40.1 us -> 7.48 us  [shards(): lax.all_gather(mix_u_weight, 'fs', axis=0, tiled=True)]
  transfers between devices with their start and end apart: 9 -> 9, of which waited for: 9 -> 9; matrix products, arithmetic and copies ran while one was open for 2% -> 3% of each run, Pallas kernels for 0% -> 0%
where the time goes in v1:
time: 582 us
  waiting for transfers between devices  512 us (88%)
  matrix products  36.2 us (6%)
  between operations  13.8 us (2%)
  other arithmetic  12.5 us (2%)
    all_gather x1, waiting for transfers between devices, shards(): lax.all_gather(gate_weight, 'fs', axis=0, tiled=True)  109 us
    all_gather x1, waiting for transfers between devices, shards(): lax.all_gather(up_weight, 'fs', axis=0, tiled=True)  107 us
    all_gather x1, waiting for transfers between devices, shards(): down_full = lax.all_gather(down_weight, 'fs', axis=1, tiled=True)  102 us
    psum x3, waiting for transfers between devices, reduce_partial(): return lax.psum(terms.astype(jnp.bfloat16), 'tp').astype(jnp.float32)  99.1 us
    all_gather x1, waiting for transfers between devices, shards(): out_full = lax.all_gather(mix_out_weight, 'fs', axis=1, tiled=True)  46.1 us
    all_to_all x1, waiting for transfers between devices, get_the_levels_all(): view_out = jax.lax.all_to_all(v1, 'fs', 0, 0)  37.9 us
    dot_general x2, matrix products, shards(): terms = jnp.dot(hidden, down_full, preferred_element_type=jnp.float32)  17.8 us
  transfers between devices with their start and end apart: 9, of which 9 were waited for; matrix products, arithmetic and copies ran while one was open for 3% of the time, Pallas kernels for 0%

profile of v1, /device:TPU:0, one launch (start us, length us, event | category | flops | bytes accessed | tf_op | source)
XLA Modules:
  0.0 581.9 jit_solution(1028414234146191270)
XLA Ops:
  6.5 0.0 copy-start.3
  6.5 0.0 all-gather.6.cloned.1.call-start
  6.5 0.7 all-gather.6.cloned.1.call-update
  7.3 0.0 all-gather.10.cloned.1.call-start
  7.3 0.7 all-gather.10.cloned.1.call-update
  8.0 0.0 all-gather.8.cloned.1.call-start
  8.1 0.7 all-gather.8.cloned.1.call-update
  8.7 0.0 all-reduce.4.cloned.1.call-start
  8.8 0.0 copy-done.3
  8.8 0.0 copy-done
  8.8 0.3 fusion.10
  9.1 109.2 %all-gather.6.cloned.1.call-done = bf16[2048,1408]{1,0:T(8,128)(2,1)} async-done(((bf16[512,1408]{1,0:T(8,128)(2,1)}), bf16[2048,1408]{1,0:T(8,128)(2,1)}) %all-gather.6.cloned.1.call-update) | async-done | bytes 5767184 | tf_op jit(solution)/shard_map/all_gather | solution.py:80
  118.3 4.5 fusion.59
  122.8 0.0 copy-start.1
  122.8 102.0 %all-gather.10.cloned.1.call-done = bf16[1408,2048]{1,0:T(8,128)(2,1)} async-done(((bf16[1408,512]{1,0:T(8,128)(2,1)}), bf16[1408,2048]{1,0:T(8,128)(2,1)}) %all-gather.10.cloned.1.call-update) | async-done | bytes 5767184 | tf_op jit(solution)/shard_map/all_gather | solution.py:83
  224.9 106.6 %all-gather.8.cloned.1.call-done = bf16[2048,1408]{1,0:T(8,128)(2,1)} async-done(((bf16[512,1408]{1,0:T(8,128)(2,1)}), bf16[2048,1408]{1,0:T(8,128)(2,1)}) %all-gather.8.cloned.1.call-update) | async-done | bytes 5767184 | tf_op jit(solution)/shard_map/all_gather | solution.py:81
  331.4 8.9 %convolution_convert_fusion.2 = bf16[256,2048]{1,0:T(8,128)(2,1)} fusion(bf16[1408,2048]{1,0:T(8,128)(2,1)} %all-gather.10.cloned.1.call-done, bf16[2048,1408]{1,0:T(8,128)(2,1)} %all-gather.8.cloned.1.call-done, f32[256,1408]{1,0:T(8,128)S(1)} %fusion.59, bf16[256,2048]{1,0:T(8,128)(2,1)S(1)} %copy-done, f32[2048]{0:T(1024)S(1)} %convert_element_type.82, ...), kind=kOutput, calls=%fused_computation.21 | convolution fusion | flops 2957574144 | bytes 15082496 | tf_op jit(solution)/shard_map/dot_general | solution.py:85
  340.4 0.0 all-reduce.4.cloned.1.call-update
  340.4 0.0 all-gather.12.cloned.1.call-start
  340.4 0.5 all-gather.12.cloned.1.call-update
  341.0 0.0 copy-done.1
  341.0 1.6 stack.2
  342.6 4.6 all-to-all-start
  347.2 0.0 all-gather.14.cloned.1.call-start
  347.2 0.5 all-gather.14.cloned.1.call-update
  347.8 0.2 all-reduce.6.cloned.1.call-start
  348.0 0.0 copy-done.4
  348.0 0.0 copy-done.5
  348.0 0.0 copy-done.9
  348.1 0.0 copy-done.10
  348.1 27.3 %all-reduce.4.cloned.1.call-done = bf16[256,2048]{1,0:T(8,128)(2,1)} async-done(((bf16[256,2048]{1,0:T(8,128)(2,1)}), bf16[256,2048]{1,0:T(8,128)(2,1)}) %all-reduce.4.cloned.1.call-update) | async-done | bytes 1048592 | tf_op jit(solution)/shard_map/psum | solution.py:27
  375.4 1.5 fusion.2
  376.9 2.0 fusion.14
  378.8 37.9 %all-to-all-done = bf16[4,512,512]{2,1,0:T(8,128)(2,1)} async-done(((bf16[4,512,512]{2,1,0:T(8,128)(2,1)}), bf16[4,512,512]{2,1,0:T(8,128)(2,1)}, u32[]{:S(2)}, u32[]{:S(2)}) %all-to-all-start) | async-done | bytes 2097184 | tf_op jit(solution)/shard_map/all_to_all | solution.py:14
  416.7 3.4 fusion.28
  420.1 0.2 reshape.105
  420.3 0.0 copy-start.2
  420.3 0.2 reshape.104
  420.5 0.3 reduce_sum.75
  420.8 0.6 multiply_reduce_fusion
  421.5 0.1 copy.36
  421.6 0.1 copy.37
  421.7 0.2 copy.25
  421.9 0.0 copy-done.2
  421.9 0.3 fusion.22
  422.2 0.2 copy.28
  422.5 7.5 %all-gather.12.cloned.1.call-done = bf16[2048,512]{1,0:T(8,128)(2,1)} async-done(((bf16[512,512]{1,0:T(8,128)(2,1)}), bf16[2048,512]{1,0:T(8,128)(2,1)}) %all-gather.12.cloned.1.call-update) | async-done | bytes 2097168 | tf_op jit(solution)/shard_map/all_gather | solution.py:89
  430.0 46.1 %all-gather.14.cloned.1.call-done = bf16[512,2048]{1,0:T(8,128)(2,1)} async-done(((bf16[512,512]{1,0:T(8,128)(2,1)}), bf16[512,2048]{1,0:T(8,128)(2,1)}) %all-gather.14.cloned.1.call-update) | async-done | bytes 2097168 | tf_op jit(solution)/shard_map/all_gather | solution.py:95
  476.0 5.7 convolution_convert_fusion
  481.7 0.0 all-reduce.6.cloned.1.call-update
  481.7 0.3 all-reduce.8.cloned.1.call-start
  482.0 0.0 copy-done.6
  482.0 0.0 copy-done.7
  482.1 34.9 %all-reduce.6.cloned.1.call-done = bf16[256,2048]{1,0:T(8,128)(2,1)} async-done(((bf16[256,2048]{1,0:T(8,128)(2,1)}), bf16[256,2048]{1,0:T(8,128)(2,1)}) %all-reduce.6.cloned.1.call-update) | async-done | bytes 1048592 | tf_op jit(solution)/shard_map/psum | solution.py:27
  517.0 1.5 fusion.5
  518.5 1.9 fusion.18
  520.4 4.5 fusion.45
  524.9 0.0 copy-start.8
  524.9 8.9 %convolution_convert_fusion.1 = bf16[256,2048]{1,0:T(8,128)(2,1)} fusion(bf16[1408,2048]{1,0:T(8,128)(2,1)} %all-gather.10.cloned.1.call-done, bf16[2048,1408]{1,0:T(8,128)(2,1)} %all-gather.8.cloned.1.call-done, f32[256,1408]{1,0:T(8,128)S(1)} %fusion.45, bf16[256,2048]{1,0:T(8,128)(2,1)S(1)} %get-tuple-element.6, f32[2048]{0:T(1024)S(1)} %convert_element_type.99, ...), kind=kOutput, calls=%fused_computation.20 | convolution fusion | flops 2957574144 | bytes 15082496 | tf_op jit(solution)/shard_map/dot_general | solution.py:100
  533.8 0.0 all-reduce.8.cloned.1.call-update
  533.9 0.0 copy-done.8
  533.9 36.9 %all-reduce.8.cloned.1.call-done = bf16[256,2048]{1,0:T(8,128)(2,1)} async-done(((bf16[256,2048]{1,0:T(8,128)(2,1)}), bf16[256,2048]{1,0:T(8,128)(2,1)}) %all-reduce.8.cloned.1.call-update) | async-done | bytes 1048592 | tf_op jit(solution)/shard_map/psum | solution.py:27
  570.8 1.5 fusion.7
  572.3 2.8 fusion.21
  (24 shorter events, 0.1 us)
Async XLA Ops:
  6.5 2.3 copy-start.3
  6.5 2.3 copy-start
  6.5 111.8 %all-gather.6.cloned.1.call-start = ((), (), s32[]{:S(2)}) async-start(), calls=%async_computation.1 | async-start | bytes 7208960 | tf_op jit(solution)/shard_map/all_gather | solution.py:80
  7.3 217.6 %all-gather.10.cloned.1.call-start = ((), (), s32[]{:S(2)}) async-start(), calls=%async_computation.3 | async-start | bytes 7208960 | tf_op jit(solution)/shard_map/all_gather | solution.py:83
  8.0 323.4 %all-gather.8.cloned.1.call-start = ((), (), s32[]{:S(2)}) async-start(), calls=%async_computation.2 | async-start | bytes 7208960 | tf_op jit(solution)/shard_map/all_gather | solution.py:81
  8.7 366.6 %all-reduce.4.cloned.1.call-start = ((), (), s32[]{:S(2)}) async-start(), calls=%async_computation.4 | async-start | bytes 2097152 | tf_op jit(solution)/shard_map/psum | solution.py:27
  122.8 218.2 %copy-start.1 = (bf16[512,512]{1,0:T(8,128)(2,1)S(1)}, bf16[512,512]{1,0:T(8,128)(2,1)}, u32[]{:S(2)}) copy-start(bf16[512,512]{1,0:T(8,128)(2,1)} %param.24) | copy-start | bytes 1572868
  340.4 89.6 %all-gather.12.cloned.1.call-start = ((), (), s32[]{:S(2)}) async-start(), calls=%async_computation.5 | async-start | bytes 2621440 | tf_op jit(solution)/shard_map/all_gather | solution.py:89
  342.6 5.4 copy-start.4
  342.6 5.4 copy-start.5
  342.6 5.5 copy-start.9
  342.6 5.5 copy-start.10
  342.6 74.1 %all-to-all-start = ((bf16[4,512,512]{2,1,0:T(8,128)(2,1)}), bf16[4,512,512]{2,1,0:T(8,128)(2,1)}, u32[]{:S(2)}, u32[]{:S(2)}) async-start(bf16[4,512,512]{2,1,0:T(8,128)(2,1)} %stack.2), calls=%async_computation | async-start | bytes 4194304 | tf_op jit(solution)/shard_map/all_to_all | solution.py:14
  347.2 128.8 %all-gather.14.cloned.1.call-start = ((), (), s32[]{:S(2)}) async-start(), calls=%async_computation.6 | async-start | bytes 2621440 | tf_op jit(solution)/shard_map/all_gather | solution.py:95
  347.8 169.3 %all-reduce.6.cloned.1.call-start = ((), (), s32[]{:S(2)}) async-start(), calls=%async_computation.7 | async-start | bytes 2097152 | tf_op jit(solution)/shard_map/psum | solution.py:27
  420.3 1.7 copy-start.2
  476.0 6.0 %copy-start.6 = (bf16[2048]{0:T(1024)(128)(2,1)S(1)}, bf16[2048]{0:T(1024)(128)(2,1)}, u32[]{:S(2)}) copy-start(bf16[2048]{0:T(1024)(128)(2,1)} %param.29) | copy-start | bytes 12292
  476.0 6.0 %copy-start.7 = (bf16[2048]{0:T(1024)(128)(2,1)S(1)}, bf16[2048]{0:T(1024)(128)(2,1)}, u32[]{:S(2)}) copy-start(bf16[2048]{0:T(1024)(128)(2,1)} %param.30) | copy-start | bytes 12292
  481.7 89.0 %all-reduce.8.cloned.1.call-start = ((), (), s32[]{:S(2)}) async-start(), calls=%async_computation.8 | async-start | bytes 2097152 | tf_op jit(solution)/shard_map/psum | solution.py:27
  524.9 9.0 %copy-start.8 = (bf16[2048]{0:T(1024)(128)(2,1)S(1)}, bf16[2048]{0:T(1024)(128)(2,1)}, u32[]{:S(2)}) copy-start(bf16[2048]{0:T(1024)(128)(2,1)} %param.31) | copy-start | bytes 12292
Sparse Core Ops, SparseCore 0:
  8.9 109.3 all-gather.5
  119.9 104.9 all-gather.9
  226.5 104.9 all-gather.7
  340.5 34.7 all-reduce.3
  376.8 53.1 all-gather.11
  431.4 44.5 all-gather.13
  481.9 35.0 all-reduce.5
  534.0 36.7 all-reduce.7
